TPU v7x, 32 devices: a whole 2x2x4 slice. The times are simulated.
32 devices in a mesh: ep: 8 (over z, x), tp: 4 (over y, core).
Axes of the slice: x: 2, y: 2, z: 4, core: 2. Of those that a mesh axis runs over, the one named last changes fastest.
Arguments:
- tokens: bfloat16 [384, 2048], P('ep', 'tp'), may hold values from -6 to 6
- conv_state: bfloat16 [384, 3, 1024], P('ep', None, 'tp'), may hold values from -6 to 6
- lru_state: float32 [384, 1024], P('ep', 'tp'), may hold values from -6 to 6
- mix_gain: float32 [2048], replicated, may hold values from 0.1 to 1.9
- input_weight: bfloat16 [2048, 1024], P(None, 'tp'), may hold values from -0.125 to 0.125
- branch_weight: bfloat16 [2048, 1024], P(None, 'tp'), may hold values from -0.125 to 0.125
- conv_taps: float32 [4, 1024], P(None, 'tp'), may hold values from -3 to 3
- conv_bias: float32 [1024], P('tp'), may hold values from -3 to 3
- recur_weight: bfloat16 [8, 128, 128], P('tp'), may hold values from -0.5 to 0.5
- recur_bias: float32 [1024], P('tp'), may hold values from -4 to 4
- inject_weight: bfloat16 [8, 128, 128], P('tp'), may hold values from -0.5 to 0.5
- inject_bias: float32 [1024], P('tp'), may hold values from -4 to 4
- decay_param: float32 [1024], P('tp'), may hold values from -1 to 4
- output_weight: bfloat16 [1024, 2048], P(None, 'tp'), may hold values from -0.1875 to 0.1875
- moe_gain: float32 [2048], replicated, may hold values from 0.1 to 1.9
- route_ids: int32 [384, 2], P('ep'), may hold values from 0 to 7, as said below
- route_logits: float32 [384, 2], P('ep'), may hold values from -6 to 6
- group_weight: float32 [384], P('ep'), may hold values from 0.25 to 1
- expert_gate: bfloat16 [8, 2048, 512], P('ep', None, 'tp'), may hold values from -0.125 to 0.125
- expert_up: bfloat16 [8, 2048, 512], P('ep', None, 'tp'), may hold values from -0.125 to 0.125
- expert_down: bfloat16 [8, 512, 2048], P('ep', 'tp'), may hold values from -0.25 to 0.25
Outputs:
- result: bfloat16 [384, 2048], P('ep', 'tp')
- new_state: float32 [384, 1024], P('ep', 'tp')
- new_conv: bfloat16 [384, 3, 1024], P('ep', None, 'tp')
Inputs may be any that keep to these rules, and one draw needn't show every extreme that they name: `route_ids`: each row names 2 different experts of one group of 4 consecutive experts (the group of expert e is e // 4). In each aligned block of 48 rows no expert is named by more than 23 rows, and in every draw some expert is named by exactly 23 rows of every block.
All inputs are finite; a program needn't handle non-finite values.
Results may differ from a plain program's by a relative error of at most 0.013.
Values may be sent and summed in bfloat16 or wider, within the bound.
A program may use at most 64 MiB of HBM per device.

v0:
```python
import jax
import jax.numpy as jnp
from jax import lax
from jax.sharding import PartitionSpec as P

PER_GROUP = 4
EPS = 1e-06
RATE = 8.0


def rms_norm(values, scales):
    wide = values.astype(jnp.float32)
    return wide * lax.rsqrt(jnp.mean(wide * wide, axis=-1, keepdims=True) + EPS) * scales


def block_gate(signal, weight, bias):
    blocks = weight.shape[0]
    grouped = signal.reshape(signal.shape[0], blocks, -1)
    mixed_out = jnp.einsum("sbi,bij->sbj", grouped, weight, preferred_element_type=jnp.float32)
    return jax.nn.sigmoid(mixed_out.reshape(signal.shape[0], -1) + bias)


def body(
    tokens,
    conv_state,
    lru_state,
    mix_gain,
    input_weight,
    branch_weight,
    conv_taps,
    conv_bias,
    recur_weight,
    recur_bias,
    inject_weight,
    inject_bias,
    decay_param,
    output_weight,
    moe_gain,
    route_ids,
    route_logits,
    group_weight,
    expert_gate,
    expert_up,
    expert_down,
):
    seq_count = tokens.shape[0]
    quarter = tokens.shape[1]
    member = lax.axis_index("tp")
    full_tokens = lax.all_gather(tokens, "tp", axis=1, tiled=True)
    model_width = full_tokens.shape[1]
    normed = rms_norm(full_tokens, mix_gain).astype(jnp.bfloat16)
    branch_x = jnp.dot(normed, input_weight, preferred_element_type=jnp.float32).astype(
        jnp.bfloat16
    )
    branch_g = jnp.dot(normed, branch_weight, preferred_element_type=jnp.float32).astype(
        jnp.bfloat16
    )
    window = jnp.concatenate([conv_state, branch_x[:, None, :]], axis=1)
    conv_sum = conv_bias + jnp.sum(window.astype(jnp.float32) * conv_taps[None], axis=1)
    conv_out = conv_sum.astype(jnp.bfloat16)
    recur_gate = block_gate(conv_out, recur_weight, recur_bias)
    inject_gate = block_gate(conv_out, inject_weight, inject_bias)
    log_rate = -RATE * recur_gate * jax.nn.softplus(-decay_param)
    new_state = jnp.exp(log_rate) * lru_state + jnp.sqrt(
        -jnp.expm1(2.0 * log_rate)
    ) * inject_gate * conv_out.astype(jnp.float32)
    mixer_out = (new_state * jax.nn.gelu(branch_g.astype(jnp.float32))).astype(jnp.bfloat16)
    mixed_out = jnp.dot(
        lax.all_gather(mixer_out, "tp", axis=1, tiled=True),
        output_weight,
        preferred_element_type=jnp.float32,
    )
    stream = (tokens.astype(jnp.float32) + mixed_out).astype(jnp.bfloat16)
    top_count = route_ids.shape[1]
    experts = lax.axis_size("ep")
    capacity = max(
        2, min((seq_count - 2) * top_count // PER_GROUP, 2 * seq_count * top_count // experts)
    )
    flat_ids = route_ids.reshape(-1)
    one_hot = (flat_ids[:, None] == jnp.arange(experts, dtype=jnp.int32)[None, :]).astype(jnp.int32)
    earlier = jnp.cumsum(one_hot, axis=0) - one_hot
    slot_rank = jnp.sum(one_hot * earlier, axis=1).reshape(seq_count, top_count)
    slot_index = route_ids * capacity + slot_rank
    targets = jnp.arange(experts * capacity, dtype=jnp.int32)
    dispatch = jnp.sum(
        (targets[:, None, None] == slot_index[None]).astype(jnp.float32), axis=2
    ).astype(jnp.bfloat16)
    raised = jnp.exp(route_logits)
    route_weight = group_weight[:, None] * raised / jnp.sum(raised, axis=1, keepdims=True)
    stream_wide = stream.astype(jnp.float32)
    squares = jnp.sum(stream_wide * stream_wide, axis=1)
    total_sq = lax.psum(squares, "tp")
    gain_part = lax.dynamic_slice_in_dim(moe_gain, member * quarter, quarter, 0)
    moe_part = (stream_wide * lax.rsqrt(total_sq / model_width + EPS)[:, None] * gain_part).astype(
        jnp.bfloat16
    )
    outgoing = jnp.dot(dispatch, moe_part, preferred_element_type=jnp.float32).astype(jnp.bfloat16)
    outgoing = outgoing.reshape(experts, capacity, quarter)
    arrived = lax.all_gather(
        lax.all_to_all(outgoing, "ep", split_axis=0, concat_axis=0, tiled=True),
        "tp",
        axis=2,
        tiled=True,
    )
    senders, slot_count, unused = arrived.shape
    flat_rows = arrived.reshape(senders * slot_count, model_width)
    gate_act = jnp.dot(flat_rows, expert_gate[0], preferred_element_type=jnp.float32)
    up_act = jnp.dot(flat_rows, expert_up[0], preferred_element_type=jnp.float32)
    hidden = (jax.nn.silu(gate_act) * up_act).astype(jnp.bfloat16)
    partial_value = jnp.dot(hidden, expert_down[0], preferred_element_type=jnp.float32)
    partial_value = partial_value.reshape(senders, slot_count, model_width)
    summed = lax.psum_scatter(
        partial_value.astype(jnp.bfloat16), "tp", scatter_dimension=2, tiled=True
    )
    returned = lax.all_to_all(summed, "ep", split_axis=0, concat_axis=0, tiled=True)
    flat_back = returned.reshape(experts * capacity, quarter)
    picked = jnp.take(flat_back, slot_index, axis=0).astype(jnp.float32)
    routed = jnp.sum(route_weight[:, :, None] * picked, axis=1)
    result = (stream.astype(jnp.float32) + routed).astype(jnp.bfloat16)
    return (result, new_state, window[:, 1:])


def solution(mesh):
    in_specs = (
        P("ep", "tp"),
        P("ep", None, "tp"),
        P("ep", "tp"),
        P(),
        P(None, "tp"),
        P(None, "tp"),
        P(None, "tp"),
        P("tp"),
        P("tp", None, None),
        P("tp"),
        P("tp", None, None),
        P("tp"),
        P("tp"),
        P(None, "tp"),
        P(),
        P("ep", None),
        P("ep", None),
        P("ep"),
        P("ep", None, "tp"),
        P("ep", None, "tp"),
        P("ep", "tp", None),
    )
    out_specs = (P("ep", "tp"), P("ep", "tp"), P("ep", None, "tp"))
    return jax.shard_map(body, mesh=mesh, in_specs=in_specs, out_specs=out_specs, check_vma=False)
```

profile of v0, /device:TPU:0, one launch (start us, length us, event | category | flops | bytes accessed | tf_op | source)
XLA Modules:
  0.0 100.6 jit_solution(4721863903514791036)
XLA Ops:
  7.3 7.2 %all_gather.9 = bf16[48,2048]{1,0:T(8,128)(2,1)S(1)} all-gather(bf16[48,512]{1,0:T(8,128)(2,1)} %param.21), channel_id=1, replica_groups=mesh['ep'=8,'tp'=4] {'tp'}, dimensions={1}, use_global_device_ids=true | all-gather | bytes 245760 | tf_op jit(solution)/shard_map/all_gather | solution.py:49
  14.6 0.1 fusion.9
  14.7 1.7 %fusion.4 = bf16[48,1,256]{2,0,1:T(8,128)(2,1)S(1)} fusion(bf16[2048,256]{1,0:T(8,128)(2,1)} %param.25, bf16[48,2048]{1,0:T(8,128)(2,1)S(1)} %all_gather.9, f32[2048]{0:T(1024)} %param.24, f32[48]{0:T(128)S(1)} %add_rsqrt_fusion.1), kind=kOutput, calls=%fused_computation.13 | convolution fusion | flops 50737152 | bytes 1278144 | tf_op jit(solution)/shard_map/dot_general | solution.py:52
  16.5 0.1 convolution_bitcast_fusion
  16.6 0.1 convolution_bitcast_fusion.1
  17.0 0.3 fusion.27
  17.3 5.3 %all_gather.10 = bf16[48,1024]{1,0:T(8,128)(2,1)S(1)} all-gather(bf16[48,256]{1,0:T(8,128)(2,1)S(1)} %fusion.27), channel_id=1, replica_groups=mesh['ep'=8,'tp'=4] {'tp'}, dimensions={1}, use_global_device_ids=true | all-gather | bytes 122880 | tf_op jit(solution)/shard_map/all_gather | solution.py:69
  22.7 0.4 multiply_reduce_fusion.2
  23.1 7.3 %psum.7 = f32[48]{0:T(128)S(1)} all-reduce(f32[48]{0:T(128)S(1)} %get-tuple-element.5), channel_id=1, replica_groups=mesh['ep'=8,'tp'=4] {'tp'}, use_global_device_ids=true, to_apply=%region_7.8 | all-reduce | flops 48 | bytes 384 | tf_op jit(solution)/shard_map/psum | solution.py:92
  30.5 0.1 eq.28
  30.7 0.1 reduce_window_sum.11
  30.8 0.2 select_reduce_fusion
  31.0 0.1 reshape.62
  31.3 0.8 dynamic_slice.3
  32.1 0.3 convolution_convert_fusion.1
  32.4 13.4 %all_to_all.10 = bf16[8,23,512]{2,1,0:T(8,128)(2,1)S(1)} all-to-all(bf16[8,23,512]{2,1,0:T(8,128)(2,1)S(1)} %reshape.63), channel_id=1, replica_groups=mesh['ep'=8,'tp'=4] {'ep'}, dimensions={0} | all-to-all | bytes 376832 | tf_op jit(solution)/shard_map/all_to_all | solution.py:100
  45.8 7.7 %all_gather.11 = bf16[8,23,2048]{2,1,0:T(8,128)(2,1)S(1)} all-gather(bf16[8,23,512]{2,1,0:T(8,128)(2,1)S(1)} %all_to_all.10), channel_id=1, replica_groups=mesh['ep'=8,'tp'=4] {'tp'}, dimensions={2}, use_global_device_ids=true | all-gather | bytes 942080 | tf_op jit(solution)/shard_map/all_gather | solution.py:99
  53.5 0.2 reshape.64
  53.8 0.4 fusion.7
  54.2 0.7 copy-done.19
  54.8 0.4 fusion.2
  55.2 0.6 copy-done.3
  55.9 1.2 %convolution_convert_fusion = bf16[8,23,2048]{2,1,0:T(8,128)(2,1)} fusion(bf16[8,23,128]{2,1,0:T(8,128)(2,1)S(1)} %dot_general.37, bf16[1,128,2048]{2,1,0:T(8,128)(2,1)S(1)} %copy-done.3), kind=kOutput, calls=%fused_computation.1 | convolution fusion | flops 96845824 | bytes 1325056 | tf_op jit(solution)/shard_map/dot_general | solution.py:110
  57.2 21.4 %reduce-scatter.2.cloned.1.call-done = bf16[8,23,512]{2,1,0:T(8,128)(2,1)} async-done(((bf16[8,23,2048]{2,1,0:T(8,128)(2,1)}), bf16[8,23,512]{2,1,0:T(8,128)(2,1)}) %reduce-scatter.2.cloned.1.call-update) | async-done | bytes 188432 | tf_op jit(solution)/shard_map/reduce_scatter | solution.py:112
  78.6 5.5 %all-to-all-start.1 = ((bf16[8,23,512]{2,1,0:T(8,128)(2,1)}), bf16[8,23,512]{2,1,0:T(8,128)(2,1)S(1)}, u32[]{:S(2)}, u32[]{:S(2)}) async-start(bf16[8,23,512]{2,1,0:T(8,128)(2,1)} %reduce-scatter.2.cloned.1.call-done), calls=%async_computation.2 | async-start | bytes 393216 | tf_op jit(solution)/shard_map/all_to_all | solution.py:115
  84.2 0.1 reshape.68
  84.3 0.1 copy.50
  84.5 0.6 fusion.12
  85.2 6.7 %all-to-all-done.1 = bf16[8,23,512]{2,1,0:T(8,128)(2,1)S(1)} async-done(((bf16[8,23,512]{2,1,0:T(8,128)(2,1)}), bf16[8,23,512]{2,1,0:T(8,128)(2,1)S(1)}, u32[]{:S(2)}, u32[]{:S(2)}) %all-to-all-start.1) | async-done | bytes 188448 | tf_op jit(solution)/shard_map/all_to_all | solution.py:115
  92.0 0.8 gather_fusion
  92.8 0.4 multiply_reduce_fusion
  93.1 0.6 add_convert_fusion
  (60 shorter events, 1.1 us)
Async XLA Ops:
  7.2 15.5 %copy-start = (bf16[1024,512]{1,0:T(8,128)(2,1)S(1)}, bf16[1024,512]{1,0:T(8,128)(2,1)}, u32[]{:S(2)}) copy-start(bf16[1024,512]{1,0:T(8,128)(2,1)} %param.34) | copy-start | bytes 3145732
  7.2 9.2 %copy-start.4 = (bf16[48,3,256]{2,0,1:T(8,128)(2,1)S(1)}, bf16[48,3,256]{2,0,1:T(8,128)(2,1)}, u32[]{:S(2)}) copy-start(bf16[48,3,256]{2,0,1:T(8,128)(2,1)} %param.22) | copy-start | bytes 221188
  7.2 9.2 %copy-start.12 = (f32[4,256]{1,0:T(4,128)S(1)}, f32[4,256]{1,0:T(4,128)}, u32[]{:S(2)}) copy-start(f32[4,256]{1,0:T(4,128)} %param.27) | copy-start | bytes 12292
  7.2 9.3 %copy-start.11 = (f32[256]{0:T(256)S(1)}, f32[256]{0:T(256)}, u32[]{:S(2)}) copy-start(f32[256]{0:T(256)} %param.28) | copy-start | bytes 3076
  7.2 9.3 %copy-start.7 = (bf16[2,128,128]{2,1,0:T(8,128)(2,1)S(1)}, bf16[2,128,128]{2,1,0:T(8,128)(2,1)}, u32[]{:S(2)}) copy-start(bf16[2,128,128]{2,1,0:T(8,128)(2,1)} %param.31) | copy-start | bytes 196612
  7.2 9.4 %copy-start.8 = (bf16[2,128,128]{2,1,0:T(8,128)(2,1)S(1)}, bf16[2,128,128]{2,1,0:T(8,128)(2,1)}, u32[]{:S(2)}) copy-start(bf16[2,128,128]{2,1,0:T(8,128)(2,1)} %param.29) | copy-start | bytes 196612
  7.2 71.3 %reduce-scatter.2.cloned.1.call-start = ((), (), s32[]{:S(2)}) async-start(), calls=%async_computation.3 | async-start | bytes 983040 | tf_op jit(solution)/shard_map/reduce_scatter | solution.py:112
  7.3 9.5 %copy-start.17 = (f32[256]{0:T(256)S(1)}, f32[256]{0:T(256)}, u32[]{:S(2)}) copy-start(f32[256]{0:T(256)} %param.33) | copy-start | bytes 3076
  7.3 9.5 %copy-start.9 = (f32[48,256]{1,0:T(8,128)S(1)}, f32[48,256]{1,0:T(8,128)}, u32[]{:S(2)}) copy-start(f32[48,256]{1,0:T(8,128)} %param.23) | copy-start | bytes 147460
  7.3 9.5 %copy-start.14 = (f32[256]{0:T(256)S(1)}, f32[256]{0:T(256)}, u32[]{:S(2)}) copy-start(f32[256]{0:T(256)} %param.32) | copy-start | bytes 3076
  7.3 9.5 %copy-start.15 = (f32[256]{0:T(256)S(1)}, f32[256]{0:T(256)}, u32[]{:S(2)}) copy-start(f32[256]{0:T(256)} %param.30) | copy-start | bytes 3076
  14.7 2.2 %copy-start.1 = (bf16[2048,256]{1,0:T(8,128)(2,1)S(1)}, bf16[2048,256]{1,0:T(8,128)(2,1)}, u32[]{:S(2)}) copy-start(bf16[2048,256]{1,0:T(8,128)(2,1)} %param.26) | copy-start | bytes 3145732
  14.7 2.2 %copy-start.10 = (f32[2048]{0:T(1024)S(1)}, f32[2048]{0:T(1024)}, u32[]{:S(2)}) copy-start(f32[2048]{0:T(1024)} %param.24) | copy-start | bytes 24580
  16.5 6.2 %copy-start.5 = (bf16[48,512]{1,0:T(8,128)(2,1)S(1)}, bf16[48,512]{1,0:T(8,128)(2,1)}, u32[]{:S(2)}) copy-start(bf16[48,512]{1,0:T(8,128)(2,1)} %param.21) | copy-start | bytes 147460
  16.9 6.1 %copy-start.6 = (f32[48,256]{1,0:T(8,128)}, f32[48,256]{1,0:T(8,128)S(1)}, u32[]{:S(2)}) copy-start(f32[48,256]{1,0:T(8,128)S(1)} %fusion.36) | copy-start | bytes 147460
  17.0 13.4 %copy-start.13 = (s32[48,2]{0,1:T(2,128)S(1)}, s32[48,2]{0,1:T(2,128)}, u32[]{:S(2)}) copy-start(s32[48,2]{0,1:T(2,128)} %param.36) | copy-start | bytes 1156
  45.8 8.0 %copy-start.2 = (bf16[1,2048,128]{2,1,0:T(8,128)(2,1)S(1)}, bf16[1,2048,128]{2,1,0:T(8,128)(2,1)}, u32[]{:S(2)}) copy-start(bf16[1,2048,128]{2,1,0:T(8,128)(2,1)} %param.39) | copy-start | bytes 1572868
  53.8 1.0 %copy-start.19 = (bf16[1,2048,128]{2,1,0:T(8,128)(2,1)S(1)}, bf16[1,2048,128]{2,1,0:T(8,128)(2,1)}, u32[]{:S(2)}) copy-start(bf16[1,2048,128]{2,1,0:T(8,128)(2,1)} %param.40) | copy-start | bytes 1572868
  54.8 1.0 %copy-start.3 = (bf16[1,128,2048]{2,1,0:T(8,128)(2,1)S(1)}, bf16[1,128,2048]{2,1,0:T(8,128)(2,1)}, u32[]{:S(2)}) copy-start(bf16[1,128,2048]{2,1,0:T(8,128)(2,1)} %param.41) | copy-start | bytes 1572868
  55.9 1.3 %copy-start.16 = (f32[48,2]{0,1:T(2,128)S(1)}, f32[48,2]{0,1:T(2,128)}, u32[]{:S(2)}) copy-start(f32[48,2]{0,1:T(2,128)} %param.37) | copy-start | bytes 1156
  55.9 1.3 %copy-start.18 = (f32[48]{0:T(128)S(1)}, f32[48]{0:T(128)}, u32[]{:S(2)}) copy-start(f32[48]{0:T(128)} %param.38) | copy-start | bytes 580
  78.6 13.3 %all-to-all-start.1 = ((bf16[8,23,512]{2,1,0:T(8,128)(2,1)}), bf16[8,23,512]{2,1,0:T(8,128)(2,1)S(1)}, u32[]{:S(2)}, u32[]{:S(2)}) async-start(bf16[8,23,512]{2,1,0:T(8,128)(2,1)} %reduce-scatter.2.cloned.1.call-done), calls=%async_computation.2 | async-start | bytes 393216 | tf_op jit(solution)/shard_map/all_to_all | solution.py:115
Sparse Core Ops, SparseCore 0:
  57.3 21.2 reduce-scatter.1
where the time goes:
time: 101 us
  blocking collectives  41 us (41%)
  waiting for transfers between devices  28.1 us (28%)
  between operations  14.4 us (14%)
  starting transfers between devices  5.56 us (6%)
  matrix products  4.86 us (5%)
  local copies, waits for them, and re-layouts  4.23 us (4%)
  other arithmetic  2.45 us (2%)
    reduce_scatter x1, waiting for transfers between devices, body(): lax.psum_scatter(partial_value.astype(jnp.bfloat16), 'tp', scatter_dimens...  21.4 us
    all_to_all x1, blocking collectives, body(): lax.all_to_all(outgoing, 'ep', split_axis=0, concat_axis=0, tiled=True)  13.4 us
    all_gather x1, blocking collectives, body(): lax.all_gather(lax.all_to_all(outgoing, 'ep', split_axis=0, concat_axis=0...  7.74 us
    psum x1, blocking collectives, body(): total_sq = lax.psum(squares, 'tp')  7.3 us
    all_gather x1, blocking collectives, body(): full_tokens = lax.all_gather(tokens, 'tp', axis=1, tiled=True)  7.24 us
    all_to_all x1, waiting for transfers between devices, body(): lax.all_to_all(summed, 'ep', split_axis=0, concat_axis=0, tiled=True)  6.72 us
    all_to_all x1, starting transfers between devices, body(): lax.all_to_all(summed, 'ep', split_axis=0, concat_axis=0, tiled=True)  5.52 us
    all_gather x1, blocking collectives, body(): lax.all_gather(mixer_out, 'tp', axis=1, tiled=True)  5.33 us
  transfers between devices with their start and end apart: 2, of which 2 were waited for; matrix products, arithmetic and copies ran while one was open for 1% of the time, Pallas kernels for 0%

commit v1 on v0

--- a/solution.py
+++ b/solution.py
@@ -66,7 +66,7 @@
     ) * inject_gate * conv_out.astype(jnp.float32)
     mixer_out = (new_state * jax.nn.gelu(branch_g.astype(jnp.float32))).astype(jnp.bfloat16)
     mixed_out = jnp.dot(
-        lax.all_gather(mixer_out, "tp", axis=1, tiled=True),
+        jnp.concatenate(lax.all_gather(mixer_out, "tp"), axis=1),
         output_weight,
         preferred_element_type=jnp.float32,
     )

time: 101 us -> 101 us (level)
  no operation moved by 1% of the time
where the time goes in v1:
time: 101 us
  blocking collectives  41 us (41%)
  waiting for transfers between devices  28.1 us (28%)
  between operations  14.4 us (14%)
  starting transfers between devices  5.56 us (6%)
  matrix products  4.87 us (5%)
  local copies, waits for them, and re-layouts  4.3 us (4%)
  other arithmetic  2.45 us (2%)
    reduce_scatter x1, waiting for transfers between devices, body(): lax.psum_scatter(partial_value.astype(jnp.bfloat16), 'tp', scatter_dimens...  21.4 us
    all_to_all x1, blocking collectives, body(): lax.all_to_all(outgoing, 'ep', split_axis=0, concat_axis=0, tiled=True)  13.4 us
    all_gather x1, blocking collectives, body(): lax.all_gather(lax.all_to_all(outgoing, 'ep', split_axis=0, concat_axis=0...  7.73 us
    psum x1, blocking collectives, body(): total_sq = lax.psum(squares, 'tp')  7.3 us
    all_gather x1, blocking collectives, body(): full_tokens = lax.all_gather(tokens, 'tp', axis=1, tiled=True)  7.24 us
    all_to_all x1, waiting for transfers between devices, body(): lax.all_to_all(summed, 'ep', split_axis=0, concat_axis=0, tiled=True)  6.72 us
    all_to_all x1, starting transfers between devices, body(): lax.all_to_all(summed, 'ep', split_axis=0, concat_axis=0, tiled=True)  5.52 us
    all_gather x1, blocking collectives, body(): lax.all_gather(mixer_out, 'tp')  5.33 us
  transfers between devices with their start and end apart: 2, of which 2 were waited for; matrix products, arithmetic and copies ran while one was open for 1% of the time, Pallas kernels for 0%

profile of v1, /device:TPU:0, one launch (start us, length us, event | category | flops | bytes accessed | tf_op | source)
XLA Modules:
  0.0 100.7 jit_solution(14049682206985675527)
XLA Ops:
  7.3 7.2 %all_gather.12 = bf16[48,2048]{1,0:T(8,128)(2,1)S(1)} all-gather(bf16[48,512]{1,0:T(8,128)(2,1)} %param.21), channel_id=1, replica_groups=mesh['ep'=8,'tp'=4] {'tp'}, dimensions={1}, use_global_device_ids=true | all-gather | bytes 245760 | tf_op jit(solution)/shard_map/all_gather | solution.py:49
  14.6 0.1 fusion.9
  14.7 1.7 %fusion.4 = bf16[48,1,256]{2,0,1:T(8,128)(2,1)S(1)} fusion(bf16[2048,256]{1,0:T(8,128)(2,1)} %param.25, bf16[48,2048]{1,0:T(8,128)(2,1)S(1)} %all_gather.12, f32[2048]{0:T(1024)} %param.24, f32[48]{0:T(128)S(1)} %add_rsqrt_fusion.1), kind=kOutput, calls=%fused_computation.13 | convolution fusion | flops 50737152 | bytes 1278144 | tf_op jit(solution)/shard_map/dot_general | solution.py:52
  16.5 0.1 convolution_bitcast_fusion
  16.6 0.1 convolution_bitcast_fusion.1
  17.0 0.3 fusion.27
  17.3 5.3 %all-gather = bf16[192,256]{1,0:T(8,128)(2,1)S(1)} all-gather(bf16[48,256]{1,0:T(8,128)(2,1)S(1)} %fusion.27), channel_id=2, replica_groups=mesh['ep'=8,'tp'=4] {'tp'}, dimensions={0}, use_global_device_ids=true | all-gather | bytes 122880 | tf_op jit(solution)/shard_map/all_gather | solution.py:69
  22.7 0.4 multiply_reduce_fusion.2
  23.1 7.3 %psum.7 = f32[48]{0:T(128)S(1)} all-reduce(f32[48]{0:T(128)S(1)} %get-tuple-element.5), channel_id=1, replica_groups=mesh['ep'=8,'tp'=4] {'tp'}, use_global_device_ids=true, to_apply=%region_7.8 | all-reduce | flops 48 | bytes 384 | tf_op jit(solution)/shard_map/psum | solution.py:92
  30.6 0.1 eq.28
  30.8 0.1 reduce_window_sum.11
  30.9 0.2 select_reduce_fusion
  31.1 0.1 reshape.70
  31.4 0.8 dynamic_slice.3
  32.2 0.3 convolution_convert_fusion.1
  32.5 13.4 %all_to_all.10 = bf16[8,23,512]{2,1,0:T(8,128)(2,1)S(1)} all-to-all(bf16[8,23,512]{2,1,0:T(8,128)(2,1)S(1)} %reshape.71), channel_id=1, replica_groups=mesh['ep'=8,'tp'=4] {'ep'}, dimensions={0} | all-to-all | bytes 376832 | tf_op jit(solution)/shard_map/all_to_all | solution.py:100
  45.9 7.7 %all_gather.15 = bf16[8,23,2048]{2,1,0:T(8,128)(2,1)S(1)} all-gather(bf16[8,23,512]{2,1,0:T(8,128)(2,1)S(1)} %all_to_all.10), channel_id=1, replica_groups=mesh['ep'=8,'tp'=4] {'tp'}, dimensions={2}, use_global_device_ids=true | all-gather | bytes 942080 | tf_op jit(solution)/shard_map/all_gather | solution.py:99
  53.6 0.2 reshape.72
  53.9 0.4 fusion.7
  54.3 0.7 copy-done.19
  54.9 0.4 fusion.2
  55.3 0.6 copy-done.3
  56.0 1.2 %convolution_convert_fusion = bf16[8,23,2048]{2,1,0:T(8,128)(2,1)} fusion(bf16[8,23,128]{2,1,0:T(8,128)(2,1)S(1)} %dot_general.37, bf16[1,128,2048]{2,1,0:T(8,128)(2,1)S(1)} %copy-done.3), kind=kOutput, calls=%fused_computation.1 | convolution fusion | flops 96845824 | bytes 1325056 | tf_op jit(solution)/shard_map/dot_general | solution.py:110
  57.3 21.4 %reduce-scatter.2.cloned.1.call-done = bf16[8,23,512]{2,1,0:T(8,128)(2,1)} async-done(((bf16[8,23,2048]{2,1,0:T(8,128)(2,1)}), bf16[8,23,512]{2,1,0:T(8,128)(2,1)}) %reduce-scatter.2.cloned.1.call-update) | async-done | bytes 188432 | tf_op jit(solution)/shard_map/reduce_scatter | solution.py:112
  78.7 5.5 %all-to-all-start.1 = ((bf16[8,23,512]{2,1,0:T(8,128)(2,1)}), bf16[8,23,512]{2,1,0:T(8,128)(2,1)S(1)}, u32[]{:S(2)}, u32[]{:S(2)}) async-start(bf16[8,23,512]{2,1,0:T(8,128)(2,1)} %reduce-scatter.2.cloned.1.call-done), calls=%async_computation.2 | async-start | bytes 393216 | tf_op jit(solution)/shard_map/all_to_all | solution.py:115
  84.3 0.1 reshape.76
  84.4 0.1 copy.53
  84.6 0.6 fusion.12
  85.3 6.7 %all-to-all-done.1 = bf16[8,23,512]{2,1,0:T(8,128)(2,1)S(1)} async-done(((bf16[8,23,512]{2,1,0:T(8,128)(2,1)}), bf16[8,23,512]{2,1,0:T(8,128)(2,1)S(1)}, u32[]{:S(2)}, u32[]{:S(2)}) %all-to-all-start.1) | async-done | bytes 188448 | tf_op jit(solution)/shard_map/all_to_all | solution.py:115
  92.0 0.8 gather_fusion
  92.9 0.4 multiply_reduce_fusion
  93.2 0.6 add_convert_fusion
  (62 shorter events, 1.1 us)
Async XLA Ops:
  7.2 15.6 %copy-start = (bf16[1024,512]{1,0:T(8,128)(2,1)S(1)}, bf16[1024,512]{1,0:T(8,128)(2,1)}, u32[]{:S(2)}) copy-start(bf16[1024,512]{1,0:T(8,128)(2,1)} %param.34) | copy-start | bytes 3145732
  7.2 9.2 %copy-start.4 = (bf16[48,3,256]{2,0,1:T(8,128)(2,1)S(1)}, bf16[48,3,256]{2,0,1:T(8,128)(2,1)}, u32[]{:S(2)}) copy-start(bf16[48,3,256]{2,0,1:T(8,128)(2,1)} %param.22) | copy-start | bytes 221188
  7.2 9.2 %copy-start.12 = (f32[4,256]{1,0:T(4,128)S(1)}, f32[4,256]{1,0:T(4,128)}, u32[]{:S(2)}) copy-start(f32[4,256]{1,0:T(4,128)} %param.27) | copy-start | bytes 12292
  7.2 9.3 %copy-start.11 = (f32[256]{0:T(256)S(1)}, f32[256]{0:T(256)}, u32[]{:S(2)}) copy-start(f32[256]{0:T(256)} %param.28) | copy-start | bytes 3076
  7.2 9.3 %copy-start.7 = (bf16[2,128,128]{2,1,0:T(8,128)(2,1)S(1)}, bf16[2,128,128]{2,1,0:T(8,128)(2,1)}, u32[]{:S(2)}) copy-start(bf16[2,128,128]{2,1,0:T(8,128)(2,1)} %param.31) | copy-start | bytes 196612
  7.2 9.4 %copy-start.8 = (bf16[2,128,128]{2,1,0:T(8,128)(2,1)S(1)}, bf16[2,128,128]{2,1,0:T(8,128)(2,1)}, u32[]{:S(2)}) copy-start(bf16[2,128,128]{2,1,0:T(8,128)(2,1)} %param.29) | copy-start | bytes 196612
  7.2 71.4 %reduce-scatter.2.cloned.1.call-start = ((), (), s32[]{:S(2)}) async-start(), calls=%async_computation.3 | async-start | bytes 983040 | tf_op jit(solution)/shard_map/reduce_scatter | solution.py:112
  7.3 9.5 %copy-start.17 = (f32[256]{0:T(256)S(1)}, f32[256]{0:T(256)}, u32[]{:S(2)}) copy-start(f32[256]{0:T(256)} %param.33) | copy-start | bytes 3076
  7.3 9.5 %copy-start.9 = (f32[48,256]{1,0:T(8,128)S(1)}, f32[48,256]{1,0:T(8,128)}, u32[]{:S(2)}) copy-start(f32[48,256]{1,0:T(8,128)} %param.23) | copy-start | bytes 147460
  7.3 9.5 %copy-start.14 = (f32[256]{0:T(256)S(1)}, f32[256]{0:T(256)}, u32[]{:S(2)}) copy-start(f32[256]{0:T(256)} %param.32) | copy-start | bytes 3076
  7.3 9.5 %copy-start.15 = (f32[256]{0:T(256)S(1)}, f32[256]{0:T(256)}, u32[]{:S(2)}) copy-start(f32[256]{0:T(256)} %param.30) | copy-start | bytes 3076
  14.7 2.2 %copy-start.1 = (bf16[2048,256]{1,0:T(8,128)(2,1)S(1)}, bf16[2048,256]{1,0:T(8,128)(2,1)}, u32[]{:S(2)}) copy-start(bf16[2048,256]{1,0:T(8,128)(2,1)} %param.26) | copy-start | bytes 3145732
  14.7 2.2 %copy-start.10 = (f32[2048]{0:T(1024)S(1)}, f32[2048]{0:T(1024)}, u32[]{:S(2)}) copy-start(f32[2048]{0:T(1024)} %param.24) | copy-start | bytes 24580
  16.8 5.9 %copy-start.5 = (bf16[48,512]{1,0:T(8,128)(2,1)S(1)}, bf16[48,512]{1,0:T(8,128)(2,1)}, u32[]{:S(2)}) copy-start(bf16[48,512]{1,0:T(8,128)(2,1)} %param.21) | copy-start | bytes 147460
  16.9 6.2 %copy-start.6 = (f32[48,256]{1,0:T(8,128)}, f32[48,256]{1,0:T(8,128)S(1)}, u32[]{:S(2)}) copy-start(f32[48,256]{1,0:T(8,128)S(1)} %fusion.36) | copy-start | bytes 147460
  17.3 13.2 %copy-start.13 = (s32[48,2]{0,1:T(2,128)S(1)}, s32[48,2]{0,1:T(2,128)}, u32[]{:S(2)}) copy-start(s32[48,2]{0,1:T(2,128)} %param.36) | copy-start | bytes 1156
  45.9 8.0 %copy-start.2 = (bf16[1,2048,128]{2,1,0:T(8,128)(2,1)S(1)}, bf16[1,2048,128]{2,1,0:T(8,128)(2,1)}, u32[]{:S(2)}) copy-start(bf16[1,2048,128]{2,1,0:T(8,128)(2,1)} %param.39) | copy-start | bytes 1572868
  53.9 1.0 %copy-start.19 = (bf16[1,2048,128]{2,1,0:T(8,128)(2,1)S(1)}, bf16[1,2048,128]{2,1,0:T(8,128)(2,1)}, u32[]{:S(2)}) copy-start(bf16[1,2048,128]{2,1,0:T(8,128)(2,1)} %param.40) | copy-start | bytes 1572868
  54.9 1.0 %copy-start.3 = (bf16[1,128,2048]{2,1,0:T(8,128)(2,1)S(1)}, bf16[1,128,2048]{2,1,0:T(8,128)(2,1)}, u32[]{:S(2)}) copy-start(bf16[1,128,2048]{2,1,0:T(8,128)(2,1)} %param.41) | copy-start | bytes 1572868
  56.0 1.3 %copy-start.16 = (f32[48,2]{0,1:T(2,128)S(1)}, f32[48,2]{0,1:T(2,128)}, u32[]{:S(2)}) copy-start(f32[48,2]{0,1:T(2,128)} %param.37) | copy-start | bytes 1156
  56.0 1.3 %copy-start.18 = (f32[48]{0:T(128)S(1)}, f32[48]{0:T(128)}, u32[]{:S(2)}) copy-start(f32[48]{0:T(128)} %param.38) | copy-start | bytes 580
  78.7 13.3 %all-to-all-start.1 = ((bf16[8,23,512]{2,1,0:T(8,128)(2,1)}), bf16[8,23,512]{2,1,0:T(8,128)(2,1)S(1)}, u32[]{:S(2)}, u32[]{:S(2)}) async-start(bf16[8,23,512]{2,1,0:T(8,128)(2,1)} %reduce-scatter.2.cloned.1.call-done), calls=%async_computation.2 | async-start | bytes 393216 | tf_op jit(solution)/shard_map/all_to_all | solution.py:115
Sparse Core Ops, SparseCore 0:
  57.4 21.2 reduce-scatter.1
